TPU v7x, 32 devices: a whole 2x2x4 slice. The times are simulated.
32 devices in a mesh: kv: 8 (over z, x), tp: 4 (over y, core).
Axes of the slice: x: 2, y: 2, z: 4, core: 2. Of those that a mesh axis runs over, the one named last changes fastest.
Arguments:
- tokens: bfloat16 [8, 4096], P(None, 'kv'), may hold values from -15 to 15
- norm_gain: float32 [4096], P('kv'), may hold values from 0.1 to 1.9
- w_query: bfloat16 [4096, 2048], P('kv', 'tp'), may hold values from -0.09375 to 0.09375
- w_key: bfloat16 [4096, 2048], P('kv', 'tp'), may hold values from -0.09375 to 0.09375
- w_value: bfloat16 [4096, 2048], P('kv', 'tp'), may hold values from -0.09375 to 0.09375
- w_forget: bfloat16 [4096, 32], P('kv', 'tp'), may hold values from -0.09375 to 0.09375
- forget_bias: float32 [32], P('tp'), may hold values from -1 to 3
- key_cache: bfloat16 [8, 3072, 2048], P(None, 'kv', 'tp'), may hold values from -360 to 360
- value_cache: bfloat16 [8, 3072, 2048], P(None, 'kv', 'tp'), may hold values from -6 to 6
- gate_cache: float32 [8, 32, 3072], P(None, 'tp', 'kv'), may hold values from -3072 to 0, as said below
- lengths: int32 [8], replicated, may hold values from 1536 to 3072, as said below
- w_out: bfloat16 [2048, 4096], P('tp', 'kv'), may hold values from -0.125 to 0.125
Outputs:
- mixed: bfloat16 [8, 4096], P(None, ('kv', 'tp'))
- log_total: float32 [8, 32], P(None, 'tp')
Inputs may be any that keep to these rules, and one draw needn't show every extreme that they name: `lengths`: the largest length equals 3072. `gate_cache`: never increasing along positions.
All inputs are finite; a program needn't handle non-finite values.
Results may differ from a plain program's by a relative error of at most 0.014.
Values may be sent and summed in bfloat16 or wider, within the bound.
A program may use at most 64 MiB of HBM per device.

v0:
```python
import jax
import jax.numpy as jnp
from jax import lax
from jax.sharding import PartitionSpec as P

D = 4096
HEAD = 64


EPS = 1e-06
MASKED = -1e30


def combined_all(value, axis, join):
    pieces = jax.tree.map(lambda part: lax.all_gather(part, axis), value)
    head = jax.tree.map(lambda part: part[0], pieces)
    tail = jax.tree.map(lambda part: part[1:], pieces)
    total, _ = lax.scan(lambda total, piece: (join(total, piece), None), head, tail)
    return total


def combine_parts(first, second):
    top = jnp.maximum(first[0], second[0])
    left = jnp.exp(first[0] - top)
    right = jnp.exp(second[0] - top)
    return (
        top,
        first[1] * left + second[1] * right,
        first[2] * left[..., None] + second[2] * right[..., None],
        first[3] + second[3],
    )


def body(
    tokens,
    norm_gain,
    w_query,
    w_key,
    w_value,
    w_forget,
    forget_bias,
    key_cache,
    value_cache,
    gate_cache,
    lengths,
    w_out,
):
    batch = tokens.shape[0]
    heads = gate_cache.shape[1]
    positions_dev = gate_cache.shape[2]
    wide = tokens.astype(jnp.float32)
    scaled = (wide * norm_gain).astype(jnp.bfloat16)
    local_square = jnp.sum(wide * wide, axis=-1)
    part_query = jnp.dot(scaled, w_query, preferred_element_type=jnp.float32)
    part_key = jnp.dot(scaled, w_key, preferred_element_type=jnp.float32)
    part_value = jnp.dot(scaled, w_value, preferred_element_type=jnp.float32)
    part_forget = jnp.dot(scaled, w_forget, preferred_element_type=jnp.float32)
    sum_query, sum_key, sum_value, sum_forget, square_sum = lax.psum(
        (part_query, part_key, part_value, part_forget, local_square), "kv"
    )
    rstd = lax.rsqrt(square_sum / D + EPS)[:, None]
    query = (sum_query * rstd).astype(jnp.bfloat16)
    key_new = (sum_key * rstd).astype(jnp.bfloat16)
    value_new = (sum_value * rstd).astype(jnp.bfloat16)
    log_gate = jax.nn.log_sigmoid(sum_forget * rstd + forget_bias)
    positions = lax.axis_index("kv") * positions_dev + jnp.arange(positions_dev, dtype=jnp.int32)
    usable = (positions[None, :] < lengths[:, None])[:, None, :]
    last = (positions[None, :] == lengths[:, None] - 1)[:, None, :]
    local_last = jnp.sum(jnp.where(last, gate_cache, 0.0), axis=-1)
    query_heads = query.reshape(batch, heads, HEAD)
    keys_four = key_cache.reshape(batch, positions_dev, heads, HEAD)
    values_four = value_cache.reshape(batch, positions_dev, heads, HEAD)
    score = jnp.einsum(
        "bhe,bphe->bhp", query_heads, keys_four, preferred_element_type=jnp.float32
    ) * HEAD ** (-0.5)
    score = jnp.where(usable, score - gate_cache, MASKED)
    local_max = jnp.max(score, axis=-1)
    weights = jnp.where(usable, jnp.exp(score - local_max[..., None]), 0.0)
    local_sum = jnp.sum(weights, axis=-1)
    local_acc = jnp.einsum(
        "bhp,bphe->bhe",
        weights.astype(jnp.bfloat16),
        values_four,
        preferred_element_type=jnp.float32,
    )
    self_score = jnp.sum(
        query_heads.astype(jnp.float32) * key_new.reshape(batch, heads, HEAD).astype(jnp.float32),
        axis=-1,
    ) * HEAD ** (-0.5)
    cache_max, cache_sum, cache_acc, gate_last = combined_all(
        (local_max, local_sum, local_acc, local_last), "kv", combine_parts
    )
    gate_now = gate_last + log_gate
    cache_top = cache_max + gate_now
    top = jnp.maximum(cache_top, self_score)
    cache_factor = jnp.exp(cache_top - top)
    self_factor = jnp.exp(self_score - top)
    total = cache_sum * cache_factor + self_factor
    attended = (
        cache_acc * cache_factor[..., None]
        + self_factor[..., None] * value_new.reshape(batch, heads, HEAD).astype(jnp.float32)
    ) / total[..., None]
    attended = attended.reshape(batch, heads * HEAD).astype(jnp.bfloat16)
    log_total = top + jnp.log(total)
    partial_value = jnp.dot(attended, w_out, preferred_element_type=jnp.float32)
    mixed = lax.psum_scatter(
        partial_value.astype(jnp.bfloat16), "tp", scatter_dimension=1, tiled=True
    )
    return (mixed, log_total)


def solution(mesh):
    placed = (
        P(None, "kv"),
        P("kv"),
        P("kv", "tp"),
        P("kv", "tp"),
        P("kv", "tp"),
        P("kv", "tp"),
        P("tp"),
        P(None, "kv", "tp"),
        P(None, "kv", "tp"),
        P(None, "tp", "kv"),
        P(),
        P("tp", "kv"),
    )
    return jax.shard_map(
        body,
        mesh=mesh,
        in_specs=placed,
        out_specs=(P(None, ("kv", "tp")), P(None, "tp")),
        check_vma=False,
    )
```

profile of v0, /device:TPU:0, one launch (start us, length us, event | category | flops | bytes accessed | tf_op | source)
XLA Modules:
  0.0 216.7 jit_solution(13370886599869400907)
XLA Ops:
  7.2 0.9 fusion.11
  8.1 0.1 copy-done
  8.2 0.9 fusion.17
  9.1 1.3 fusion.19
  10.3 1.3 fusion.23
  11.6 0.9 fusion.21
  12.5 39.3 %all-reduce = (f32[8,512]{1,0:T(8,128)S(1)}, f32[8]{0:T(128)S(1)}, f32[8,512]{1,0:T(8,128)S(1)}, f32[8,512]{1,0:T(8,128)S(1)}, f32[8,8]{1,0:T(8,128)S(1)}) all-reduce(f32[8,512]{1,0:T(8,128)S(1)} %fusion.17, f32[8]{0:T(128)S(1)} %fusion.11, f32[8,512]{1,0:T(8,128)S(1)} %fusion.23, ...), channel_id=1, replica_groups=mesh['kv'=8,'tp'=4] {'kv'}, use_global_device_ids=true, to_apply=%region_11.12 | all-reduce | flops 12360 | bytes 98880 | tf_op jit(solution)/shard_map/psum | solution.py:58
  51.9 0.1 reshape.107
  52.0 4.7 %copy.16 = bf16[8,384,512]{1,2,0:T(8,128)(2,1)} copy(bf16[8,384,512]{2,1,0:T(8,128)(2,1)} %param.21) | data formatting | bytes 6291456 | tf_op args[7]
  56.7 4.7 %copy.17 = bf16[8,384,512]{1,2,0:T(8,128)(2,1)} copy(bf16[8,384,512]{2,1,0:T(8,128)(2,1)} %param.22) | data formatting | bytes 6291456 | tf_op args[8]
  61.4 2.7 %fusion.27 = f32[8,8,1,384]{3,2,1,0:T(1,128)S(1)} fusion(bf16[8,8,64,1]{2,3,1,0:T(2,128)(2,1)S(1)} %reshape.107, bf16[8,384,8,64]{1,3,2,0:T(8,128)(2,1)} %bitcast.57), kind=kOutput, calls=%fused_computation.53 | convolution fusion | flops 3145728 | bytes 3252224 | tf_op jit(solution)/shard_map/bhe,bphe->bhp/dot_general | solution.py:73
  64.1 0.1 fusion.25
  64.2 0.2 select_reduce_fusion
  64.4 1.2 fusion.5
  65.6 30.7 %all-gather.2 = f32[64,8,64]{2,1,0:T(8,128)S(1)} all-gather(f32[8,8,64]{2,1,0:T(8,128)S(1)} %bitcast.61), channel_id=4, replica_groups=mesh['kv'=8,'tp'=4] {'kv'}, dimensions={0}, use_global_device_ids=true | all-gather | bytes 147456 | tf_op jit(solution)/shard_map/all_gather | solution.py:15
  96.4 30.6 %all-gather.1 = f32[64,8]{1,0:T(8,128)S(1)} all-gather(f32[8,8]{1,0:T(8,128)S(1)} %get-tuple-element.57), channel_id=3, replica_groups=mesh['kv'=8,'tp'=4] {'kv'}, dimensions={0}, use_global_device_ids=true | all-gather | bytes 2304 | tf_op jit(solution)/shard_map/all_gather | solution.py:15
  127.0 30.6 %all-gather.3 = f32[64,8]{1,0:T(8,128)S(1)} all-gather(f32[8,8]{1,0:T(8,128)S(1)} %get-tuple-element.56), channel_id=5, replica_groups=mesh['kv'=8,'tp'=4] {'kv'}, dimensions={0}, use_global_device_ids=true | all-gather | bytes 2304 | tf_op jit(solution)/shard_map/all_gather | solution.py:15
  157.6 30.6 %all-gather = f32[64,8]{1,0:T(8,128)S(1)} all-gather(f32[8,8]{1,0:T(8,128)S(1)} %fusion.25), channel_id=2, replica_groups=mesh['kv'=8,'tp'=4] {'kv'}, dimensions={0}, use_global_device_ids=true | all-gather | bytes 2304 | tf_op jit(solution)/shard_map/all_gather | solution.py:15
  188.3 0.9 while.16
  188.3 0.1 fusion.40
  188.4 0.1 fusion.40
  188.6 0.1 fusion.40
  188.7 0.1 fusion.40
  188.8 0.1 fusion.40
  189.0 0.1 fusion.40
  189.5 0.7 log_add_fusion
  190.2 0.1 divide_convert_fusion
  190.3 0.1 convert_element_type.54
  190.4 0.2 convolution_convert_fusion
  190.5 0.8 copy.22
  191.3 17.1 %reduce-scatter.4.cloned.1.call-done = bf16[128,8]{1,0:T(8,128)(2,1)} async-done(((bf16[512,8]{1,0:T(8,128)(2,1)}), bf16[128,8]{1,0:T(8,128)(2,1)}) %reduce-scatter.4.cloned.1.call-update) | async-done | bytes 2064
  208.4 1.4 copy.23
  (38 shorter events, 0.8 us)
Async XLA Ops:
  7.2 1.1 copy-start
  7.2 201.3 %reduce-scatter.4.cloned.1.call-start = ((), (), s32[]{:S(2)}) async-start(), calls=%async_computation.1 | async-start | bytes 163840
  52.0 4.7 %copy-start.5 = (s32[8]{0:T(128)S(1)}, s32[8]{0:T(128)}, u32[]{:S(2)}) copy-start(s32[8]{0:T(128)} %param.24) | copy-start | bytes 100
  61.3 2.8 %copy-start.3 = (f32[8,8,384]{2,1,0:T(8,128)S(1)}, f32[8,8,384]{2,1,0:T(8,128)}, u32[]{:S(2)}) copy-start(f32[8,8,384]{2,1,0:T(8,128)} %param.23) | copy-start | bytes 294916
  61.3 3.1 %copy-start.1 = (bf16[8,384,512]{1,2,0:T(8,128)(2,1)S(1)}, bf16[8,384,512]{1,2,0:T(8,128)(2,1)}, u32[]{:S(2)}) copy-start(bf16[8,384,512]{1,2,0:T(8,128)(2,1)} %copy.17) | copy-start | bytes 9437188
  64.0 125.4 %copy-start.4 = (f32[8]{0:T(128)S(1)}, f32[8]{0:T(128)}, u32[]{:S(2)}) copy-start(f32[8]{0:T(128)} %param.20) | copy-start | bytes 100
  64.0 126.3 %copy-start.2 = (bf16[512,512]{1,0:T(8,128)(2,1)S(1)}, bf16[512,512]{1,0:T(8,128)(2,1)}, u32[]{:S(2)}) copy-start(bf16[512,512]{1,0:T(8,128)(2,1)} %param.25) | copy-start | bytes 1572868
Sparse Core Ops, SparseCore 0:
  191.5 16.9 reduce-scatter.3
where the time goes:
time: 217 us
  blocking collectives  162 us (75%)
  waiting for transfers between devices  17.1 us (8%)
  between operations  14.1 us (6%)
  local copies, waits for them, and re-layouts  12.2 us (6%)
  matrix products  8.27 us (4%)
  other arithmetic  2.94 us (1%)
    all_gather x4, blocking collectives, combined_all(): pieces = jax.tree.map(lambda part: lax.all_gather(part, axis), value)  123 us
    psum x1, blocking collectives, body(): lax.psum((part_query, part_key, part_value, part_forget, local_square), '...  39.3 us
    unnamed x2, waiting for transfers between devices  17.1 us
    unnamed x16, local copies, waits for them, and re-layouts  11.7 us
  transfers between devices with their start and end apart: 1, of which 1 were waited for; matrix products, arithmetic and copies ran while one was open for 0% of the time, Pallas kernels for 0%

commit v1 on v0

v1 whole, which is shorter than its diff:
```python
import functools

import jax
import jax.numpy as jnp
from jax import lax
from jax.experimental import pallas as pl
from jax.experimental.pallas import tpu as pltpu
from jax.sharding import PartitionSpec as P

EPS = 1e-06
MASKED = -1e30
F32 = jnp.float32
BF16 = jnp.bfloat16


def exchange(axis, me, n, buf, send_sem, recv_sem):
    for d in range(1, n):
        pltpu.make_async_remote_copy(
            src_ref=buf.at[me],
            dst_ref=buf.at[me],
            send_sem=send_sem.at[d - 1],
            recv_sem=recv_sem.at[d - 1],
            device_id={axis: lax.rem(me + d, n)},
            device_id_type=pl.DeviceIdType.MESH,
        ).start()


def arrived(axis, me, n, buf, send_sem, recv_sem):
    for d in range(1, n):
        slot = lax.rem(me + n - d, n)
        pltpu.make_async_remote_copy(
            src_ref=buf.at[slot],
            dst_ref=buf.at[slot],
            send_sem=send_sem.at[d - 1],
            recv_sem=recv_sem.at[d - 1],
            device_id={axis: slot},
            device_id_type=pl.DeviceIdType.MESH,
        ).wait_recv()


def left(axis, me, n, buf, send_sem, recv_sem):
    for d in range(1, n):
        pltpu.make_async_remote_copy(
            src_ref=buf.at[me],
            dst_ref=buf.at[me],
            send_sem=send_sem.at[d - 1],
            recv_sem=recv_sem.at[d - 1],
            device_id={axis: lax.rem(me + d, n)},
            device_id_type=pl.DeviceIdType.MESH,
        ).wait_send()


def kernel(n, t, features, lengths, tokens_h, gain_h, wq_h, wk_h, wv_h, wf_h, bias_h, key_h, value_h, gate_h, wo_h,
           mixed, log_total, tokens, gain, wq, wk, wv, wf, bias, key, value, gate, wo,
           proj, pval, stats, acc, outs, inbox,
           in_sem, proj_s, proj_r, pval_s, pval_r, stats_s, stats_r, acc_s, acc_r, out_s, out_r):
    me = lax.axis_index("kv")
    mt = lax.axis_index("tp")
    batch, heads, positions = gate.shape
    width = wq.shape[1]
    size = width // heads

    pairs = [(tokens_h, tokens), (gain_h, gain), (wq_h, wq), (wf_h, wf), (wv_h, wv), (wk_h, wk), (gate_h, gate),
             (bias_h, bias), (key_h, key), (value_h, value), (wo_h, wo)]
    copies = [pltpu.make_async_copy(a, b, in_sem.at[i]) for i, (a, b) in enumerate(pairs)]
    (c_tok, c_gain, c_wq, c_wf, c_wv, c_wk, c_gate, c_bias, c_key, c_value, c_wo) = copies
    for c in copies:
        c.start()

    barrier = pltpu.get_barrier_semaphore()
    for d in range(1, n):
        pl.semaphore_signal(barrier, inc=1, device_id={"kv": lax.rem(me + d, n)}, device_id_type=pl.DeviceIdType.MESH)
    for d in range(1, t):
        pl.semaphore_signal(barrier, inc=1, device_id={"tp": lax.rem(mt + d, t)}, device_id_type=pl.DeviceIdType.MESH)

    c_tok.wait()
    c_gain.wait()
    wide = tokens[...].astype(F32)
    scaled = (wide * gain[...]).astype(BF16)
    square = jnp.sum(wide * wide, axis=-1, keepdims=True)
    c_wq.wait()
    c_wf.wait()
    proj[me, :, :width] = jnp.dot(scaled, wq[...], preferred_element_type=F32)
    proj[me, :, width:] = jnp.broadcast_to(square, (batch, 128))
    proj[me, :, width : width + heads] = lax.dot_general(
        scaled, wf[...], (((1,), (1,)), ((), ())), preferred_element_type=F32)
    pl.semaphore_wait(barrier, n - 1 + t - 1)
    proj_x = ("kv", me, n, proj, proj_s, proj_r)
    exchange(*proj_x)

    c_wv.wait()
    pval[me] = jnp.dot(scaled, wv[...], preferred_element_type=F32).astype(BF16)
    pval_x = ("kv", me, n, pval, pval_s, pval_r)
    exchange(*pval_x)
    c_wk.wait()
    part_key = jnp.dot(scaled, wk[...], preferred_element_type=F32)
    c_gate.wait()
    c_bias.wait()
    c_key.wait()

    arrived(*proj_x)
    summed = jnp.sum(proj[...], axis=0)
    rstd = lax.rsqrt(summed[:, width + heads : width + heads + 1] / features + EPS)
    query = (summed[:, :width] * rstd).astype(BF16).astype(F32)
    forget = summed[:, width : width + heads] * rstd + bias[...]
    log_gate = jnp.minimum(forget, 0.0) - jnp.log1p(jnp.exp(-jnp.abs(forget)))

    row = lax.broadcasted_iota(jnp.int32, (heads, width), 0)
    col = lax.broadcasted_iota(jnp.int32, (heads, width), 1)
    own = (col >= row * size) & (col < (row + 1) * size)
    place = me * positions + lax.broadcasted_iota(jnp.int32, (heads, positions), 1)
    h_row = lax.broadcasted_iota(jnp.int32, (heads, 128), 0)
    lane = lax.broadcasted_iota(jnp.int32, (heads, 128), 1)
    scale = size ** -0.5
    c_value.wait()
    rows, sums = [], []
    for b in range(batch):
        spread = jnp.where(own, query[b : b + 1, :], 0.0)
        score = lax.dot_general(spread.astype(BF16), key[b], (((1,), (1,)), ((), ())), preferred_element_type=F32) * scale
        g = gate[b]
        usable = place < lengths[b]
        score = jnp.where(usable, score - g, MASKED)
        top = jnp.max(score, axis=-1, keepdims=True)
        weights = jnp.where(usable, jnp.exp(score - top), 0.0)
        total = jnp.sum(weights, axis=-1, keepdims=True)
        last = jnp.sum(jnp.where(place == lengths[b] - 1, g, 0.0), axis=-1, keepdims=True)
        own_score = jnp.sum(spread * part_key[b : b + 1, :], axis=-1, keepdims=True)
        tile = jnp.where(lane == h_row, top, 0.0)
        tile = jnp.where(lane == h_row + heads, total, tile)
        tile = jnp.where(lane == h_row + 2 * heads, last, tile)
        tile = jnp.where(lane == h_row + 3 * heads, own_score, tile)
        sums.append(jnp.sum(tile, axis=0, keepdims=True))
        full = jnp.dot(weights.astype(BF16), value[b], preferred_element_type=F32)
        rows.append(jnp.sum(jnp.where(own, full, 0.0), axis=0, keepdims=True))
    stats[me] = jnp.concatenate(sums, axis=0)
    acc[me] = jnp.concatenate(rows, axis=0).astype(BF16)
    stats_x = ("kv", me, n, stats, stats_s, stats_r)
    acc_x = ("kv", me, n, acc, acc_s, acc_r)
    exchange(*stats_x)
    exchange(*acc_x)

    arrived(*pval_x)
    value_new = jnp.sum(pval[...].astype(F32), axis=0)
    arrived(*stats_x)
    st = stats[...]
    tops = st[:, :, :heads]
    cache_max = jnp.max(tops, axis=0)
    factor = jnp.exp(tops - cache_max[None])
    cache_sum = jnp.sum(factor * st[:, :, heads : 2 * heads], axis=0)
    gate_now = jnp.sum(st[:, :, 2 * heads : 3 * heads], axis=0) + log_gate
    self_score = jnp.sum(st[:, :, 3 * heads : 4 * heads], axis=0) * rstd * scale
    cache_top = cache_max + gate_now
    top = jnp.maximum(cache_top, self_score)
    cache_factor = jnp.exp(cache_top - top)
    self_factor = jnp.exp(self_score - top)
    total = cache_sum * cache_factor + self_factor
    log_total[...] = top + jnp.log(total)
    inverse = 1.0 / total
    each = factor * (cache_factor * inverse)[None]
    coef = jnp.concatenate([each.reshape(n * batch, heads), self_factor * inverse * rstd], axis=0)
    wide_coef = jnp.dot(coef, own.astype(F32), precision=lax.Precision.HIGHEST, preferred_element_type=F32)
    arrived(*acc_x)
    attended = wide_coef[n * batch :] * value_new + jnp.sum(
        wide_coef[: n * batch].reshape(n, batch, width) * acc[...].astype(F32), axis=0)
    c_wo.wait()
    partial = jnp.dot(attended.astype(BF16), wo[...], preferred_element_type=F32).astype(BF16)
    cols = partial.shape[1] // t
    for i in range(t):
        outs[i] = partial[:, i * cols : (i + 1) * cols]
    for d in range(1, t):
        peer = lax.rem(mt + d, t)
        pltpu.make_async_remote_copy(
            src_ref=outs.at[peer], dst_ref=inbox.at[mt], send_sem=out_s.at[d - 1], recv_sem=out_r.at[d - 1],
            device_id={"tp": peer}, device_id_type=pl.DeviceIdType.MESH).start()
    inbox[mt] = outs[mt]
    left(*proj_x)
    left(*pval_x)
    left(*stats_x)
    left(*acc_x)
    for d in range(1, t):
        slot = lax.rem(mt + t - d, t)
        pltpu.make_async_remote_copy(
            src_ref=outs.at[slot], dst_ref=inbox.at[slot], send_sem=out_s.at[d - 1], recv_sem=out_r.at[d - 1],
            device_id={"tp": slot}, device_id_type=pl.DeviceIdType.MESH).wait()
    mixed[...] = jnp.sum(inbox[...].astype(F32), axis=0).astype(BF16)


def body(n, t, tokens, norm_gain, w_query, w_key, w_value, w_forget, forget_bias, key_cache, value_cache, gate_cache,
         lengths, w_out):
    batch = tokens.shape[0]
    heads = gate_cache.shape[1]
    width = w_query.shape[1]
    cols = w_out.shape[1] // t
    arrays = (tokens, norm_gain.reshape(1, -1), w_query, w_key, w_value, w_forget.T, forget_bias.reshape(1, -1),
              key_cache, value_cache, gate_cache, w_out)
    dma = pltpu.SemaphoreType.DMA
    return pl.pallas_call(
        functools.partial(kernel, n, t, float(tokens.shape[1] * n)),
        out_shape=(
            jax.ShapeDtypeStruct((batch, cols), BF16),
            jax.ShapeDtypeStruct((batch, heads), F32),
        ),
        in_specs=[pl.BlockSpec(memory_space=pltpu.SMEM)] + [pl.BlockSpec(memory_space=pl.ANY)] * len(arrays),
        out_specs=(pl.BlockSpec(memory_space=pltpu.VMEM), pl.BlockSpec(memory_space=pltpu.VMEM)),
        scratch_shapes=[pltpu.VMEM(a.shape, a.dtype) for a in arrays] + [
            pltpu.VMEM((n, batch, width + 128), F32),
            pltpu.VMEM((n, batch, width), BF16),
            pltpu.VMEM((n, batch, 128), F32),
            pltpu.VMEM((n, batch, width), BF16),
            pltpu.VMEM((t, batch, cols), BF16),
            pltpu.VMEM((t, batch, cols), BF16),
            dma((len(arrays),)),
        ] + [dma((n - 1,))] * 8 + [dma((t - 1,))] * 2,
        compiler_params=pltpu.CompilerParams(collective_id=0, has_side_effects=True),
    )(lengths, *arrays)


def solution(mesh):
    placed = (
        P(None, "kv"),
        P("kv"),
        P("kv", "tp"),
        P("kv", "tp"),
        P("kv", "tp"),
        P("kv", "tp"),
        P("tp"),
        P(None, "kv", "tp"),
        P(None, "kv", "tp"),
        P(None, "tp", "kv"),
        P(),
        P("tp", "kv"),
    )
    return jax.shard_map(
        functools.partial(body, mesh.shape["kv"], mesh.shape["tp"]),
        mesh=mesh,
        in_specs=placed,
        out_specs=(P(None, ("kv", "tp")), P(None, "tp")),
        check_vma=False,
    )
```

time: 217 us -> 28.5 us (0.13)
  blocking collectives: 162 us -> 0 us
  Pallas kernels: 0 us -> 25 us
  waiting for transfers between devices: 17.1 us -> 0 us
  between operations: 14.1 us -> 0.64 us
  local copies, waits for them, and re-layouts: 12.2 us -> 2.5 us
  matrix products: 8.27 us -> 0 us
  other arithmetic: 2.94 us -> 0 us
    all_gather x4 -> x0, blocking collectives: 123 us -> none  [combined_all(): pieces = jax.tree.map(lambda part: lax.all_gather(part, axis), value)]
    psum x1 -> x0, blocking collectives: 39.3 us -> none  [body(): lax.psum((part_query, part_key, part_value, part_forget, local_square), '...]
    pallas_call x0 -> x1, Pallas kernels: none -> 25 us  [body(): pl.pallas_call(functools.partial(kernel, n, t, float(tokens.shape[1] * n)...]
    unnamed x2 -> x0, waiting for transfers between devices: 17.1 us -> none
    unnamed x16 -> x2, local copies, waits for them, and re-layouts: 11.7 us -> 2.5 us
    dot_general x7 -> x0, matrix products: 8.27 us -> none  [the longest x1 2.68 us: body(): jnp.einsum('bhe,bphe->bhp', query_heads, keys_four, preferred_element_typ...]
  transfers between devices with their start and end apart: 1 -> 0, of which waited for: 1 -> 0; matrix products, arithmetic and copies ran while one was open for 0% -> 0% of each run, Pallas kernels for 0% -> 0%
where the time goes in v1:
time: 28.5 us; the launch traced here: 28.2 us
  Pallas kernels  25 us (88%)
  local copies, waits for them, and re-layouts  2.5 us (9%)
  between operations  0.64 us (2%)
    pallas_call x1, Pallas kernels, body(): pl.pallas_call(functools.partial(kernel, n, t, float(tokens.shape[1] * n)...  25 us
    unnamed x2, local copies, waits for them, and re-layouts  2.5 us

profile of v1, /device:TPU:0, one launch (start us, length us, event | category | flops | bytes accessed | tf_op | source)
XLA Modules:
  0.0 28.2 jit_solution(13174491993803901426)
XLA Ops:
  0.6 25.0 %shard_map.131 = (bf16[8,128]{1,0:T(8,128)(2,1)}, f32[8,8]{1,0:T(8,128)}) custom-call(s32[8]{0:T(128)} %lengths.1, bf16[8,512]{1,0:T(8,128)(2,1)} %tokens_h.1, f32[1,512]{1,0:T(1,128)} %bitcast.4, bf16[512,512]{1,0:T(8,128)(2,1)} %wq_h.1, bf16[512,512]{1,0:T(8,128)(2,1)} %wk_h.1, bf16[512,512]{1,0:T(8,128)(2,1)} %wv_h.1, bf16[8,512]{1,0:T(8,128)(2,1)} %bitcast.3, ...), custom_call_target="tpu_custom_call" | custom-call | tf_op jit(solution)/shard_map/pallas_call | solution.py:197
  25.7 1.2 %copy.16 = bf16[8,128]{1,0:T(8,128)(2,1)} copy(bf16[8,128]{1,0:T(8,128)(2,1)} %get-tuple-element.4) | data formatting | bytes 4096
  26.9 1.3 %copy.17 = f32[8,8]{1,0:T(8,128)} copy(f32[8,8]{1,0:T(8,128)} %get-tuple-element.5) | data formatting | bytes 512

commit v2 on v1

--- a/solution.py
+++ b/solution.py
@@ -51,8 +51,8 @@
 
 
 def kernel(n, t, features, lengths, tokens_h, gain_h, wq_h, wk_h, wv_h, wf_h, bias_h, key_h, value_h, gate_h, wo_h,
-           mixed, log_total, tokens, gain, wq, wk, wv, wf, bias, key, value, gate, wo,
-           proj, pval, stats, acc, outs, inbox,
+           inbox, logs, tokens, gain, wq, wk, wv, wf, bias, key, value, gate, wo,
+           proj, pval, stats, acc, outs,
            in_sem, proj_s, proj_r, pval_s, pval_r, stats_s, stats_r, acc_s, acc_r, out_s, out_r):
     me = lax.axis_index("kv")
     mt = lax.axis_index("tp")
@@ -64,14 +64,15 @@
              (bias_h, bias), (key_h, key), (value_h, value), (wo_h, wo)]
     copies = [pltpu.make_async_copy(a, b, in_sem.at[i]) for i, (a, b) in enumerate(pairs)]
     (c_tok, c_gain, c_wq, c_wf, c_wv, c_wk, c_gate, c_bias, c_key, c_value, c_wo) = copies
-    for c in copies:
-        c.start()
-
     barrier = pltpu.get_barrier_semaphore()
     for d in range(1, n):
         pl.semaphore_signal(barrier, inc=1, device_id={"kv": lax.rem(me + d, n)}, device_id_type=pl.DeviceIdType.MESH)
     for d in range(1, t):
         pl.semaphore_signal(barrier, inc=1, device_id={"tp": lax.rem(mt + d, t)}, device_id_type=pl.DeviceIdType.MESH)
+
+    for c in (c_tok, c_gain, c_wq, c_wf):
+        c.start()
+    late = (c_wv, c_wk, c_gate, c_bias, c_key, c_value, c_wo)
 
     c_tok.wait()
     c_gain.wait()
@@ -80,6 +81,8 @@
     square = jnp.sum(wide * wide, axis=-1, keepdims=True)
     c_wq.wait()
     c_wf.wait()
+    for c in late:
+        c.start()
     proj[me, :, :width] = jnp.dot(scaled, wq[...], preferred_element_type=F32)
     proj[me, :, width:] = jnp.broadcast_to(square, (batch, 128))
     proj[me, :, width : width + heads] = lax.dot_general(
@@ -154,7 +157,7 @@
     cache_factor = jnp.exp(cache_top - top)
     self_factor = jnp.exp(self_score - top)
     total = cache_sum * cache_factor + self_factor
-    log_total[...] = top + jnp.log(total)
+    logs[...] = top + jnp.log(total)
     inverse = 1.0 / total
     each = factor * (cache_factor * inverse)[None]
     coef = jnp.concatenate([each.reshape(n * batch, heads), self_factor * inverse * rstd], axis=0)
@@ -182,7 +185,11 @@
         pltpu.make_async_remote_copy(
             src_ref=outs.at[slot], dst_ref=inbox.at[slot], send_sem=out_s.at[d - 1], recv_sem=out_r.at[d - 1],
             device_id={"tp": slot}, device_id_type=pl.DeviceIdType.MESH).wait()
+
+
+def finish(inbox, logs, mixed, log_total):
     mixed[...] = jnp.sum(inbox[...].astype(F32), axis=0).astype(BF16)
+    log_total[...] = logs[...]
 
 
 def body(n, t, tokens, norm_gain, w_query, w_key, w_value, w_forget, forget_bias, key_cache, value_cache, gate_cache,
@@ -194,25 +201,31 @@
     arrays = (tokens, norm_gain.reshape(1, -1), w_query, w_key, w_value, w_forget.T, forget_bias.reshape(1, -1),
               key_cache, value_cache, gate_cache, w_out)
     dma = pltpu.SemaphoreType.DMA
-    return pl.pallas_call(
+    vmem = pl.BlockSpec(memory_space=pltpu.VMEM)
+    inbox, logs = pl.pallas_call(
         functools.partial(kernel, n, t, float(tokens.shape[1] * n)),
         out_shape=(
-            jax.ShapeDtypeStruct((batch, cols), BF16),
+            jax.ShapeDtypeStruct((t, batch, cols), BF16),
             jax.ShapeDtypeStruct((batch, heads), F32),
         ),
         in_specs=[pl.BlockSpec(memory_space=pltpu.SMEM)] + [pl.BlockSpec(memory_space=pl.ANY)] * len(arrays),
-        out_specs=(pl.BlockSpec(memory_space=pltpu.VMEM), pl.BlockSpec(memory_space=pltpu.VMEM)),
+        out_specs=(vmem, vmem),
         scratch_shapes=[pltpu.VMEM(a.shape, a.dtype) for a in arrays] + [
             pltpu.VMEM((n, batch, width + 128), F32),
             pltpu.VMEM((n, batch, width), BF16),
             pltpu.VMEM((n, batch, 128), F32),
             pltpu.VMEM((n, batch, width), BF16),
             pltpu.VMEM((t, batch, cols), BF16),
-            pltpu.VMEM((t, batch, cols), BF16),
             dma((len(arrays),)),
         ] + [dma((n - 1,))] * 8 + [dma((t - 1,))] * 2,
         compiler_params=pltpu.CompilerParams(collective_id=0, has_side_effects=True),
     )(lengths, *arrays)
+    return pl.pallas_call(
+        finish,
+        out_shape=(jax.ShapeDtypeStruct((batch, cols), BF16), jax.ShapeDtypeStruct((batch, heads), F32)),
+        in_specs=[vmem, vmem],
+        out_specs=(vmem, vmem),
+    )(inbox, logs)
 
 
 def solution(mesh):

time: 28.5 us -> 27.3 us (0.958)
  local copies, waits for them, and re-layouts: 2.5 us -> 0 us
  Pallas kernels: 25 us -> 26.4 us
    unnamed x2 -> x0, local copies, waits for them, and re-layouts: 2.5 us -> none
    pallas_call x0 -> x1, Pallas kernels: none -> 1.3 us  [body(): pl.pallas_call(finish, out_shape=(jax.ShapeDtypeStruct((batch, cols), BF1...]
where the time goes in v2:
time: 27.3 us; the launch traced here: 27 us
  Pallas kernels  26.4 us (97%)
  between operations  0.64 us (2%)
    pallas_call x1, Pallas kernels, body(): pl.pallas_call(functools.partial(kernel, n, t, float(tokens.shape[1] * n)...  25.1 us
    pallas_call x1, Pallas kernels, body(): pl.pallas_call(finish, out_shape=(jax.ShapeDtypeStruct((batch, cols), BF1...  1.3 us

profile of v2, /device:TPU:0, one launch (start us, length us, event | category | flops | bytes accessed | tf_op | source)
XLA Modules:
  0.0 27.0 jit_solution(2828945609695305171)
XLA Ops:
  0.6 25.1 %shard_map.131 = (bf16[4,8,128]{2,1,0:T(8,128)(2,1)}, f32[8,8]{1,0:T(8,128)}) custom-call(s32[8]{0:T(128)} %lengths.1, bf16[8,512]{1,0:T(8,128)(2,1)} %tokens_h.1, f32[1,512]{1,0:T(1,128)} %bitcast.4, bf16[512,512]{1,0:T(8,128)(2,1)} %wq_h.1, bf16[512,512]{1,0:T(8,128)(2,1)} %wk_h.1, bf16[512,512]{1,0:T(8,128)(2,1)} %wv_h.1, bf16[8,512]{1,0:T(8,128)(2,1)} %bitcast.3, ...), custom_call_target="tpu_custom_call" | custom-call | tf_op jit(solution)/shard_map/pallas_call | solution.py:205
  25.7 1.3 %shard_map.132 = (bf16[8,128]{1,0:T(8,128)(2,1)}, f32[8,8]{1,0:T(8,128)}) custom-call(bf16[4,8,128]{2,1,0:T(8,128)(2,1)} %get-tuple-element.4.inbox, f32[8,8]{1,0:T(8,128)} %get-tuple-element.5.logs), custom_call_target="tpu_custom_call" | custom-call | tf_op jit(solution)/shard_map/pallas_call | solution.py:223

commit v3 on v2

--- a/solution.py
+++ b/solution.py
@@ -14,7 +14,7 @@
 
 
 def exchange(axis, me, n, buf, send_sem, recv_sem):
-    for d in range(1, n):
+    for d in sorted(range(1, n), key=lambda d: -min(d, n - d)):
         pltpu.make_async_remote_copy(
             src_ref=buf.at[me],
             dst_ref=buf.at[me],
@@ -94,7 +94,6 @@
     c_wv.wait()
     pval[me] = jnp.dot(scaled, wv[...], preferred_element_type=F32).astype(BF16)
     pval_x = ("kv", me, n, pval, pval_s, pval_r)
-    exchange(*pval_x)
     c_wk.wait()
     part_key = jnp.dot(scaled, wk[...], preferred_element_type=F32)
     c_gate.wait()
@@ -102,6 +101,7 @@
     c_key.wait()
 
     arrived(*proj_x)
+    exchange(*pval_x)
     summed = jnp.sum(proj[...], axis=0)
     rstd = lax.rsqrt(summed[:, width + heads : width + heads + 1] / features + EPS)
     query = (summed[:, :width] * rstd).astype(BF16).astype(F32)
@@ -115,8 +115,7 @@
     h_row = lax.broadcasted_iota(jnp.int32, (heads, 128), 0)
     lane = lax.broadcasted_iota(jnp.int32, (heads, 128), 1)
     scale = size ** -0.5
-    c_value.wait()
-    rows, sums = [], []
+    rows, sums, lows = [], [], []
     for b in range(batch):
         spread = jnp.where(own, query[b : b + 1, :], 0.0)
         score = lax.dot_general(spread.astype(BF16), key[b], (((1,), (1,)), ((), ())), preferred_element_type=F32) * scale
@@ -133,13 +132,16 @@
         tile = jnp.where(lane == h_row + 2 * heads, last, tile)
         tile = jnp.where(lane == h_row + 3 * heads, own_score, tile)
         sums.append(jnp.sum(tile, axis=0, keepdims=True))
-        full = jnp.dot(weights.astype(BF16), value[b], preferred_element_type=F32)
+        lows.append(weights.astype(BF16))
+    stats[me] = jnp.concatenate(sums, axis=0)
+    stats_x = ("kv", me, n, stats, stats_s, stats_r)
+    exchange(*stats_x)
+    c_value.wait()
+    for b in range(batch):
+        full = jnp.dot(lows[b], value[b], preferred_element_type=F32)
         rows.append(jnp.sum(jnp.where(own, full, 0.0), axis=0, keepdims=True))
-    stats[me] = jnp.concatenate(sums, axis=0)
     acc[me] = jnp.concatenate(rows, axis=0).astype(BF16)
-    stats_x = ("kv", me, n, stats, stats_s, stats_r)
     acc_x = ("kv", me, n, acc, acc_s, acc_r)
-    exchange(*stats_x)
     exchange(*acc_x)
 
     arrived(*pval_x)

time: 27.3 us -> 25 us (0.916)
  Pallas kernels: 26.4 us -> 24.1 us
    pallas_call x1, Pallas kernels: 25.1 us -> 22.8 us  [body(): pl.pallas_call(functools.partial(kernel, n, t, float(tokens.shape[1] * n)...]
where the time goes in v3:
time: 25 us; the launch traced here: 24.7 us
  Pallas kernels  24.1 us (96%)
  between operations  0.64 us (3%)
    pallas_call x1, Pallas kernels, body(): pl.pallas_call(functools.partial(kernel, n, t, float(tokens.shape[1] * n)...  22.8 us
    pallas_call x1, Pallas kernels, body(): pl.pallas_call(finish, out_shape=(jax.ShapeDtypeStruct((batch, cols), BF1...  1.3 us

profile of v3, /device:TPU:0, one launch (start us, length us, event | category | flops | bytes accessed | tf_op | source)
XLA Modules:
  0.0 24.7 jit_solution(5472107009998927111)
XLA Ops:
  0.6 22.8 %shard_map.131 = (bf16[4,8,128]{2,1,0:T(8,128)(2,1)}, f32[8,8]{1,0:T(8,128)}) custom-call(s32[8]{0:T(128)} %lengths.1, bf16[8,512]{1,0:T(8,128)(2,1)} %tokens_h.1, f32[1,512]{1,0:T(1,128)} %bitcast.4, bf16[512,512]{1,0:T(8,128)(2,1)} %wq_h.1, bf16[512,512]{1,0:T(8,128)(2,1)} %wk_h.1, bf16[512,512]{1,0:T(8,128)(2,1)} %wv_h.1, bf16[8,512]{1,0:T(8,128)(2,1)} %bitcast.3, ...), custom_call_target="tpu_custom_call" | custom-call | tf_op jit(solution)/shard_map/pallas_call | solution.py:207
  23.4 1.3 %shard_map.132 = (bf16[8,128]{1,0:T(8,128)(2,1)}, f32[8,8]{1,0:T(8,128)}) custom-call(bf16[4,8,128]{2,1,0:T(8,128)(2,1)} %get-tuple-element.4.inbox, f32[8,8]{1,0:T(8,128)} %get-tuple-element.5.logs), custom_call_target="tpu_custom_call" | custom-call | tf_op jit(solution)/shard_map/pallas_call | solution.py:225

commit v4 on v3

--- a/solution.py
+++ b/solution.py
@@ -99,6 +99,16 @@
     c_gate.wait()
     c_bias.wait()
     c_key.wait()
+    row = lax.broadcasted_iota(jnp.int32, (heads, width), 0)
+    col = lax.broadcasted_iota(jnp.int32, (heads, width), 1)
+    own = (col >= row * size) & (col < (row + 1) * size)
+    place = me * positions + lax.broadcasted_iota(jnp.int32, (heads, positions), 1)
+    h_row = lax.broadcasted_iota(jnp.int32, (heads, 128), 0)
+    lane = lax.broadcasted_iota(jnp.int32, (heads, 128), 1)
+    scale = size ** -0.5
+    lasts = [
+        jnp.sum(jnp.where(place == lengths[b] - 1, gate[b], 0.0), axis=-1, keepdims=True) for b in range(batch)
+    ]
 
     arrived(*proj_x)
     exchange(*pval_x)
@@ -108,28 +118,24 @@
     forget = summed[:, width : width + heads] * rstd + bias[...]
     log_gate = jnp.minimum(forget, 0.0) - jnp.log1p(jnp.exp(-jnp.abs(forget)))
 
-    row = lax.broadcasted_iota(jnp.int32, (heads, width), 0)
-    col = lax.broadcasted_iota(jnp.int32, (heads, width), 1)
-    own = (col >= row * size) & (col < (row + 1) * size)
-    place = me * positions + lax.broadcasted_iota(jnp.int32, (heads, positions), 1)
-    h_row = lax.broadcasted_iota(jnp.int32, (heads, 128), 0)
-    lane = lax.broadcasted_iota(jnp.int32, (heads, 128), 1)
-    scale = size ** -0.5
     rows, sums, lows = [], [], []
+    spreads = [jnp.where(own, query[b : b + 1, :], 0.0) for b in range(batch)]
+    scores = [
+        lax.dot_general(spreads[b].astype(BF16), key[b], (((1,), (1,)), ((), ())), preferred_element_type=F32) * scale
+        for b in range(batch)
+    ]
     for b in range(batch):
-        spread = jnp.where(own, query[b : b + 1, :], 0.0)
-        score = lax.dot_general(spread.astype(BF16), key[b], (((1,), (1,)), ((), ())), preferred_element_type=F32) * scale
+        spread, score = spreads[b], scores[b]
         g = gate[b]
         usable = place < lengths[b]
         score = jnp.where(usable, score - g, MASKED)
         top = jnp.max(score, axis=-1, keepdims=True)
         weights = jnp.where(usable, jnp.exp(score - top), 0.0)
         total = jnp.sum(weights, axis=-1, keepdims=True)
-        last = jnp.sum(jnp.where(place == lengths[b] - 1, g, 0.0), axis=-1, keepdims=True)
         own_score = jnp.sum(spread * part_key[b : b + 1, :], axis=-1, keepdims=True)
         tile = jnp.where(lane == h_row, top, 0.0)
         tile = jnp.where(lane == h_row + heads, total, tile)
-        tile = jnp.where(lane == h_row + 2 * heads, last, tile)
+        tile = jnp.where(lane == h_row + 2 * heads, lasts[b], tile)
         tile = jnp.where(lane == h_row + 3 * heads, own_score, tile)
         sums.append(jnp.sum(tile, axis=0, keepdims=True))
         lows.append(weights.astype(BF16))

time: 25 us -> 25 us (level)
  no operation moved by 1% of the time
where the time goes in v4:
time: 25 us; the launch traced here: 24.7 us
  Pallas kernels  24.1 us (96%)
  between operations  0.64 us (3%)
    pallas_call x1, Pallas kernels, body(): pl.pallas_call(functools.partial(kernel, n, t, float(tokens.shape[1] * n)...  22.8 us
    pallas_call x1, Pallas kernels, body(): pl.pallas_call(finish, out_shape=(jax.ShapeDtypeStruct((batch, cols), BF1...  1.3 us

profile of v4, /device:TPU:0, one launch (start us, length us, event | category | flops | bytes accessed | tf_op | source)
XLA Modules:
  0.0 24.7 jit_solution(11963547412875124280)
XLA Ops:
  0.6 22.8 %shard_map.131 = (bf16[4,8,128]{2,1,0:T(8,128)(2,1)}, f32[8,8]{1,0:T(8,128)}) custom-call(s32[8]{0:T(128)} %lengths.1, bf16[8,512]{1,0:T(8,128)(2,1)} %tokens_h.1, f32[1,512]{1,0:T(1,128)} %bitcast.4, bf16[512,512]{1,0:T(8,128)(2,1)} %wq_h.1, bf16[512,512]{1,0:T(8,128)(2,1)} %wk_h.1, bf16[512,512]{1,0:T(8,128)(2,1)} %wv_h.1, bf16[8,512]{1,0:T(8,128)(2,1)} %bitcast.3, ...), custom_call_target="tpu_custom_call" | custom-call | tf_op jit(solution)/shard_map/pallas_call | solution.py:213
  23.4 1.3 %shard_map.132 = (bf16[8,128]{1,0:T(8,128)(2,1)}, f32[8,8]{1,0:T(8,128)}) custom-call(bf16[4,8,128]{2,1,0:T(8,128)(2,1)} %get-tuple-element.4.inbox, f32[8,8]{1,0:T(8,128)} %get-tuple-element.5.logs), custom_call_target="tpu_custom_call" | custom-call | tf_op jit(solution)/shard_map/pallas_call | solution.py:231
